TPU v7x, 32 devices: a whole 2x2x4 slice. The times are simulated.
32 devices in a mesh: sp: 8 (over z, x), tp: 4 (over y, core).
Axes of the slice: x: 2, y: 2, z: 4, core: 2. Of those that a mesh axis runs over, the one named last changes fastest.
Arguments:
- tokens: bfloat16 [6144, 2048], P(('sp', 'tp')), may hold values from -6 to 6
- in_gain: float32 [2048], replicated, may hold values from 0.1 to 1.9
- w_query: bfloat16 [2048, 1024], P(None, 'tp'), may hold values from -0.125 to 0.125
- w_key: bfloat16 [2048, 1024], P(None, 'tp'), may hold values from -0.125 to 0.125
- w_value: bfloat16 [2048, 2048], P(None, 'tp'), may hold values from -0.125 to 0.125
- w_input_gate: bfloat16 [2048, 8], replicated, may hold values from -8 to 8
- w_forget_gate: bfloat16 [2048, 8], replicated, may hold values from -0.125 to 0.125
- forget_bias: float32 [8], replicated
- forget_extra: float32 [6144, 8], P('sp', 'tp'), may hold values from -2 to 0
- w_conv_gate: bfloat16 [2048, 2048], P(None, 'tp'), may hold values from -0.125 to 0.125
- w_conv_left: bfloat16 [2048, 2048], P(None, 'tp'), may hold values from -0.125 to 0.125
- w_conv_right: bfloat16 [2048, 2048], P(None, 'tp'), may hold values from -0.125 to 0.125
- conv_taps: float32 [3, 2048], replicated, may hold values from -3.5 to 3.5
- first_memory: float32 [8, 128, 256], P('tp'), may hold values from -2560 to 2560
- first_norm: float32 [8, 128], P('tp'), may hold values from -2560 to 2560
- w_out_memory: bfloat16 [2048, 2048], P('tp'), may hold values from -0.09375 to 0.09375
- w_out_conv: bfloat16 [2048, 2048], P('tp'), may hold values from -0.09375 to 0.09375
Outputs:
- mixed: bfloat16 [6144, 2048], P(('sp', 'tp'))
All inputs are finite; a program needn't handle non-finite values.
Results may differ from a plain program's by a relative error of at most 0.015.
The roundings to bfloat16 on the way count: a program that leaves them out, or rounds other values in their place, can miss the bound.
Values may be sent and summed in bfloat16 or wider, within the bound.
No kernel may reach another device: no remote copies, remote signals or barrier semaphores. Data moves between devices by JAX's collectives and lax.ppermute only.
A program may use at most 64 MiB of HBM per device.

v0:
```python
import jax
import jax.numpy as jnp
from jax import lax
from jax.sharding import PartitionSpec as P

KEY_DIM = 128
VALUE_DIM = 256
TAPS = 3
V_WIDTH = 2048


epsilon = 1e-06
very_negative = -1e30
highest = lax.Precision.HIGHEST


def from_behind(block, axis, distance):
    devices = range(lax.axis_size(axis))
    route = [(i - distance, i) for i in devices if i - distance in devices]
    return lax.ppermute(block, axis, route)


def entering(part, axis, combine, identity):
    place = lax.axis_index(axis)
    gathered = jax.tree.map(lambda a: lax.all_gather(a, axis), part)
    state = jax.tree.map(lambda a, e: jnp.zeros_like(a) + jnp.asarray(e, a.dtype), part, identity)

    def one(turn, state):
        return combine(
            state, jax.tree.map(lambda a: lax.dynamic_index_in_dim(a, turn, 0, False), gathered)
        )

    return lax.fori_loop(0, place, one, state)


def rounded(values):
    return lax.optimization_barrier(values.astype(jnp.bfloat16)).astype(jnp.float32)


def join_states(earlier, later):
    decay_early, max_early, memory_early, norm_early = earlier
    decay_late, max_late, memory_late, norm_late = later
    joined_max = jnp.maximum(max_early + decay_late, max_late)
    scale_early = jnp.exp(max_early + decay_late - joined_max)
    scale_late = jnp.exp(max_late - joined_max)
    joined_memory = (
        scale_early[:, None, None] * memory_early + scale_late[:, None, None] * memory_late
    )
    joined_norm = scale_early[:, None] * norm_early + scale_late[:, None] * norm_late
    return (decay_early + decay_late, joined_max, joined_memory, joined_norm)


def per_device(
    tokens,
    in_gain,
    w_query,
    w_key,
    w_value,
    w_input_gate,
    w_forget_gate,
    forget_bias,
    forget_extra,
    w_conv_gate,
    w_conv_left,
    w_conv_right,
    conv_taps,
    first_memory,
    first_norm,
    w_out_memory,
    w_out_conv,
):
    heads_here = w_query.shape[1] // KEY_DIM
    query_width = heads_here * KEY_DIM
    value_width = heads_here * VALUE_DIM
    channels = w_conv_gate.shape[1]
    head_first = lax.axis_index("tp") * heads_here
    channel_first = lax.axis_index("tp") * channels
    input_gate = lax.dynamic_slice_in_dim(w_input_gate, head_first, heads_here, 1)
    forget_gate = lax.dynamic_slice_in_dim(w_forget_gate, head_first, heads_here, 1)
    bias_here = lax.dynamic_slice_in_dim(forget_bias, head_first, heads_here, 0)
    taps_here = lax.dynamic_slice_in_dim(conv_taps, channel_first, channels, 1)
    token_rows = tokens.astype(jnp.float32)
    scale_rows = lax.rsqrt(jnp.mean(token_rows * token_rows, axis=1, keepdims=True) + epsilon)
    normed = (token_rows * scale_rows * in_gain).astype(jnp.bfloat16)
    sub_rows = lax.all_gather(normed, "tp", axis=0, tiled=True)
    pieces = [
        jnp.dot(sub_rows, weight, preferred_element_type=jnp.float32)
        for weight in (
            w_query,
            w_key,
            w_value,
            w_conv_gate,
            w_conv_left,
            w_conv_right,
            input_gate,
            forget_gate,
        )
    ]
    projected = jnp.concatenate(pieces, axis=1)
    row_count = projected.shape[0]
    offset_value = 2 * query_width
    offset_conv = offset_value + value_width
    offset_gate = offset_conv + 3 * channels
    query_rows = (
        projected[:, 0:query_width].astype(jnp.bfloat16).reshape(row_count, heads_here, KEY_DIM)
    )
    key_rows = (
        projected[:, query_width:offset_value]
        .astype(jnp.bfloat16)
        .reshape(row_count, heads_here, KEY_DIM)
    )
    value_rows = (
        projected[:, offset_value:offset_conv]
        .astype(jnp.bfloat16)
        .reshape(row_count, heads_here, VALUE_DIM)
    )
    conv_gate = rounded(projected[:, offset_conv : offset_conv + channels])
    conv_left = rounded(projected[:, offset_conv + channels : offset_conv + 2 * channels])
    conv_right = rounded(projected[:, offset_conv + 2 * channels : offset_gate])
    in_pre = projected[:, offset_gate : offset_gate + heads_here]
    forget_pre = projected[:, offset_gate + heads_here : offset_gate + 2 * heads_here] + bias_here
    log_forget = jax.nn.log_sigmoid(forget_pre) + forget_extra
    cumulative = jnp.cumsum(log_forget, axis=0)
    decay_total = cumulative[row_count - 1]
    weight_log = decay_total[None, :] - cumulative + in_pre
    block_max = jnp.max(weight_log, axis=0)
    keyed = key_rows.astype(jnp.float32) * jnp.exp(weight_log - block_max[None, :])[:, :, None]
    block_norm = jnp.sum(keyed, axis=0)
    block_memory = jnp.einsum(
        "shd,shv->hdv", keyed.astype(jnp.bfloat16), value_rows, preferred_element_type=jnp.float32
    )
    product = (conv_left * conv_right).astype(jnp.bfloat16)
    edge_rows = product[row_count - (TAPS - 1) :]
    before_rows = from_behind(edge_rows, "sp", 1)
    prior_decay, prior_max, prior_memory, prior_norm = entering(
        (decay_total, block_max, block_memory, block_norm),
        "sp",
        join_states,
        (
            jnp.zeros_like(decay_total),
            jnp.full_like(block_max, very_negative),
            jnp.zeros_like(block_memory),
            jnp.zeros_like(block_norm),
        ),
    )
    enter_max = jnp.maximum(prior_max, prior_decay)
    from_prior = jnp.exp(prior_max - enter_max)
    from_first = jnp.exp(prior_decay - enter_max)
    carry_memory = (
        from_prior[:, None, None] * prior_memory + from_first[:, None, None] * first_memory
    )
    carry_norm = from_prior[:, None] * prior_norm + from_first[:, None] * first_norm
    query_scale = KEY_DIM ** (-0.5)
    row_ids = lax.iota(jnp.int32, row_count)
    causal = row_ids[:, None] >= row_ids[None, :]
    cum_heads = cumulative.T
    log_gap = cum_heads[:, :, None] - cum_heads[:, None, :] + in_pre.T[:, None, :]
    log_gap = jnp.where(causal[None], log_gap, -jnp.inf)
    inter_log = cum_heads + enter_max[:, None]
    row_max = jnp.maximum(inter_log, jnp.max(log_gap, axis=2))
    raw_scores = (
        jnp.einsum("thd,shd->hts", query_rows, key_rows, preferred_element_type=jnp.float32)
        * query_scale
    )
    mixing = raw_scores * jnp.exp(log_gap - row_max[:, :, None])
    carried = jnp.exp(inter_log - row_max).T
    scaled_query = query_rows.astype(jnp.float32) * query_scale
    from_values = jnp.einsum(
        "hts,shv->thv", mixing.astype(jnp.bfloat16), value_rows, preferred_element_type=jnp.float32
    )
    from_memory = jnp.einsum("thd,hdv->thv", scaled_query, carry_memory, precision=highest)
    from_norm = jnp.einsum("thd,hd->th", scaled_query, carry_norm, precision=highest)
    numerator = from_values + carried[:, :, None] * from_memory
    denominator = jnp.sum(mixing, axis=2).T + carried * from_norm
    memory_out = numerator / jnp.maximum(jnp.abs(denominator), 1.0)[:, :, None]
    local_squares = jnp.sum(memory_out * memory_out, axis=(1, 2))
    row_total = lax.psum(local_squares, "tp")
    row_scale = lax.rsqrt(row_total / V_WIDTH + epsilon)
    heads_out = memory_out * row_scale[:, None, None]
    heads_out = heads_out.reshape(row_count, value_width).astype(jnp.bfloat16)
    padded = jnp.concatenate([before_rows, product], axis=0).astype(jnp.float32)
    filtered = taps_here[0][None, :] * padded[0:row_count]
    for tap_index in range(1, TAPS):
        filtered = (
            filtered + taps_here[tap_index][None, :] * padded[tap_index : tap_index + row_count]
        )
    conv_branch = (conv_gate * filtered).astype(jnp.bfloat16)
    return lax.psum_scatter(
        (
            jnp.dot(heads_out, w_out_memory, preferred_element_type=jnp.float32)
            + jnp.dot(conv_branch, w_out_conv, preferred_element_type=jnp.float32)
        ).astype(jnp.bfloat16),
        "tp",
        scatter_dimension=0,
        tiled=True,
    )


def solution(mesh):
    in_specs = (
        P(("sp", "tp"), None),
        P(),
        P(None, "tp"),
        P(None, "tp"),
        P(None, "tp"),
        P(),
        P(),
        P(),
        P("sp", "tp"),
        P(None, "tp"),
        P(None, "tp"),
        P(None, "tp"),
        P(),
        P("tp", None, None),
        P("tp", None),
        P("tp", None),
        P("tp", None),
    )
    out_specs = P(("sp", "tp"), None)
    return jax.shard_map(
        per_device, mesh=mesh, in_specs=in_specs, out_specs=out_specs, check_vma=False
    )
```

profile of v0, /device:TPU:0, one launch (start us, length us, event | category | flops | bytes accessed | tf_op | source)
XLA Modules:
  0.0 204.8 jit_solution(13238146320118617703)
XLA Ops:
  6.5 1.5 fusion.13
  8.1 2.3 %fusion.15 = bf16[192,2048]{1,0:T(8,128)(2,1)} fusion(bf16[192,2048]{1,0:T(8,128)(2,1)} %param.19, f32[2048]{0:T(1024)} %param.20, f32[192]{0:T(256)S(1)} %add_rsqrt_fusion.1), kind=kLoop, calls=%fused_computation.26 | loop fusion | flops 1572864 | bytes 1581824 | tf_op jit(solution)/shard_map/convert_element_type | solution.py:84
  10.5 31.2 %all-gather.6.cloned.1.call-done = bf16[768,2048]{1,0:T(8,128)(2,1)} async-done(((bf16[192,2048]{1,0:T(8,128)(2,1)}), bf16[768,2048]{1,0:T(8,128)(2,1)}) %all-gather.6.cloned.1.call-update) | async-done | bytes 3145744 | tf_op jit(solution)/shard_map/all_gather | solution.py:85
  41.8 2.8 %fusion.43 = f32[2,768]{1,0:T(2,128)S(1)} fusion(f32[768,2]{0,1:T(2,128)S(1)} %copy-done.11, bf16[768,2048]{1,0:T(8,128)(2,1)} %all-gather.6.cloned.1.call-done, bf16[2048,8]{0,1:T(8,128)(2,1)} %param.25, s32[]{:T(128)S(6)} %select_n.26, f32[2]{0:T(128)S(1)} %dynamic_slice.28), kind=kOutput, calls=%fused_computation.74 | convolution fusion | flops 6306816 | bytes 3166220 | tf_op jit(solution)/shard_map/dot_general | solution.py:87
  44.6 0.6 reduce-window.6
  45.8 3.1 %fusion.56 = (f32[2]{0:T(128)S(1)}, f32[768,2]{0,1:T(2,128)S(1)}, f32[768,2]{0,1:T(2,128)S(1)}) fusion(f32[2,768]{1,0:T(2,128)S(1)} %bitcast.127, f32[2]{0:T(128)S(1)} %slice_reduce_fusion.1, bf16[768,2048]{1,0:T(8,128)(2,1)} %all-gather.6.cloned.1.call-done, bf16[2048,8]{0,1:T(8,128)(2,1)} %param.24, s32[]{:T(128)S(6)} %select_n.26), kind=kOutput, calls=%fused_computation.97 | convolution fusion | flops 6296062 | bytes 3172372 | tf_op jit(solution)/shard_map/dot_general | solution.py:87
  49.0 0.3 copy-done.13
  49.3 1.9 convolution_convert_fusion.3
  51.2 1.1 fusion.24
  52.4 0.7 copy-done.5
  53.1 1.1 fusion.29
  54.3 0.6 dynamic-slice
  55.4 0.9 constant_dynamic-slice_fusion.2
  56.7 20.5 %all-gather.2 = f32[8,1,2]{2,1,0:T(1,128)S(1)} all-gather(f32[1,1,2]{2,1,0:T(1,128)S(1)} %bitcast.139), channel_id=1, replica_groups=mesh['sp'=8,'tp'=4] {'sp'}, dimensions={0}, use_global_device_ids=true | all-gather | bytes 72 | tf_op jit(solution)/shard_map/all_gather | solution.py:25
  77.2 17.7 %all-reduce = f32[16]{0:T(128)S(1)} all-reduce(f32[16]{0:T(128)S(1)} %dynamic-update-slice), channel_id=2, replica_groups=mesh['sp'=8,'tp'=4] {'sp'}, use_global_device_ids=true, to_apply=%add | all-reduce | flops 16 | bytes 128
  95.0 3.3 %convolution_convert_fusion.5 = bf16[768,256]{0,1:T(8,128)(2,1)S(1)} fusion(bf16[768,2048]{1,0:T(8,128)(2,1)} %all-gather.6.cloned.1.call-done, bf16[2048,256]{1,0:T(8,128)(2,1)} %param.21), kind=kOutput, calls=%fused_computation.45 | convolution fusion | flops 805502976 | bytes 4587520 | tf_op jit(solution)/shard_map/dot_general | solution.py:87
  98.6 4.5 %convolution_convert_fusion = bf16[768,512]{1,0:T(8,128)(2,1)S(1)} fusion(bf16[768,2048]{1,0:T(8,128)(2,1)} %all-gather.6.cloned.1.call-done, bf16[2048,512]{1,0:T(8,128)(2,1)} %param.30), kind=kOutput, calls=%fused_computation.40 | convolution fusion | flops 1611005952 | bytes 6029312 | tf_op jit(solution)/shard_map/dot_general | solution.py:87
  103.1 1.8 convolution_convert_fusion.1
  105.1 3.9 %collective-permute-start = (bf16[2,512]{1,0:T(2,128)(2,1)S(1)}, bf16[2,512]{1,0:T(2,128)(2,1)S(1)}, u32[]{:S(2)}, u32[]{:S(2)}) collective-permute-start(bf16[2,512]{1,0:T(2,128)(2,1)S(1)} %slice.42), channel_id=1, source_target_pairs={{0,4},{4,8},{8,12},{12,16},{16,20},{20,24},{24,28},{1,5},{5,9},{9,... | collective-permute-start | bytes 6152 | tf_op jit(solution)/shard_map/ppermute | solution.py:20
  109.1 2.7 %convolution_convert_fusion.2 = bf16[768,512]{1,0:T(8,128)(2,1)} fusion(bf16[768,2048]{1,0:T(8,128)(2,1)S(1)} %copy-done.2, bf16[2048,512]{1,0:T(8,128)(2,1)S(1)} %copy-done.15), kind=kOutput, calls=%fused_computation.42 | convolution fusion | flops 1611005952 | bytes 6029312 | tf_op jit(solution)/shard_map/dot_general | solution.py:87
  111.8 0.9 fusion.7
  112.7 16.5 %all_gather.31 = f32[8,2,128]{2,1,0:T(2,128)S(1)} all-gather(f32[1,2,128]{2,1,0:T(2,128)S(1)} %bitcast.142), channel_id=1, replica_groups=mesh['sp'=8,'tp'=4] {'sp'}, dimensions={0}, use_global_device_ids=true | all-gather | bytes 9216 | tf_op jit(solution)/shard_map/all_gather | solution.py:25
  129.2 1.4 maximum_convert_fusion
  130.8 3.4 %fusion.8 = (f32[2,768]{1,0:T(2,128)S(1)}, f32[2,768,768]{1,2,0:T(8,128)S(1)}) fusion(f32[2,768]{1,0:T(2,128)S(1)} %add_maximum_fusion, f32[2,768]{1,0:T(2,128)S(1)} %bitcast.132, f32[2,768]{1,0:T(2,128)S(1)} %bitcast.129, pred[768,768]{0,1:T(8,128)(4,1)S(1)} %iota_compare_fusion, bf16[768,2,128]{0,2,1:T(8,128)(2,1)} %bitcast.126, ...), kind=kOutput, calls=%fused_computation.17 | convolution fusion | flops 310245888 | bytes 6119424 | tf_op jit(solution)/shard_map/thd,shd->hts/dot_general | solution.py:162
  134.2 2.2 %fusion.10 = f32[2,256,768]{2,1,0:T(8,128)S(1)} fusion(bf16[768,2,256]{0,2,1:T(8,128)(2,1)S(1)} %bitcast.124, f32[2,768,768]{1,2,0:T(8,128)S(1)} %get-tuple-element.131, f32[2,768]{1,0:T(2,128)S(1)} %add_maximum_fusion, f32[2,768]{1,0:T(2,128)S(1)} %bitcast.133, f32[2,768]{1,0:T(2,128)S(1)} %bitcast.130, pred[768,768]{0,1:T(8,128)(4,1)S(1)} %iota_compare_fusion), kind=kOutput, calls=%fused_computation.20 | convolution fusion | flops 612237312 | bytes 7686144 | tf_op jit(solution)/shard_map/hts,shv->thv/dot_general | solution.py:168
  136.5 0.7 fusion.28
  137.4 2.9 %multiply_reduce_fusion = (f32[768]{0:T(1024)S(1)}, f32[768,2,256]{0,2,1:T(8,128)}) fusion(f32[768,2]{0,1:T(2,128)S(1)} %get-tuple-element.117, bf16[768,2,128]{2,0,1:T(8,128)(2,1)S(1)} %copy.40, f32[2,128,256]{2,1,0:T(8,128)S(1)} %copy-done.16, f32[2,128,256]{2,1,0:T(8,128)S(1)} %get-tuple-element.63, f32[2]{0:T(128)S(1)} %subtract_exponential_fusion.3, ...), kind=kOutput, calls=%fused_computation.39 | convolution fusion | flops 606534912 | bytes 4078608 | tf_op jit(solution)/shard_map/thd,hdv->thv/dot_general | solution.py:171
  140.3 5.9 %psum.7 = f32[768]{0:T(1024)S(1)} all-reduce(f32[768]{0:T(1024)S(1)} %get-tuple-element.132), channel_id=1, replica_groups=mesh['sp'=8,'tp'=4] {'tp'}, use_global_device_ids=true, to_apply=%region_10.11 | all-reduce | flops 768 | bytes 6144 | tf_op jit(solution)/shard_map/psum | solution.py:177
  146.1 1.5 multiply_convert_fusion.1
  147.7 1.9 fusion.57
  149.9 3.8 %add_convert_fusion = bf16[768,2048]{1,0:T(8,128)(2,1)} fusion(f32[768,2048]{1,0:T(8,128)S(1)} %fusion.57, bf16[512,2048]{1,0:T(8,128)(2,1)S(1)} %copy-done.4, f32[770,512]{1,0:T(8,128)S(1)} %copy-done.3, bf16[768,512]{1,0:T(8,128)(2,1)S(1)} %copy-done.9, f32[512]{0:T(512)S(1)} %bitcast.137, f32[512]{0:T(512)S(1)} %bitcast.136, f32[512]{0:T(512)S(1)} %bitcast.135), kind=kOutput, calls=%fused_computation.13 | convolution fusion | flops 1616904192 | bytes 17045504 | tf_op jit(solution)/shard_map/dot_general | solution.py:191
  153.7 44.5 %reduce-scatter.2.cloned.1.call-done = bf16[192,2048]{1,0:T(8,128)(2,1)} async-done(((bf16[768,2048]{1,0:T(8,128)(2,1)}), bf16[192,2048]{1,0:T(8,128)(2,1)}) %reduce-scatter.2.cloned.1.call-update) | async-done | bytes 786448 | tf_op jit(solution)/shard_map/reduce_scatter | solution.py:188
  (72 shorter events, 2.6 us)
Async XLA Ops:
  6.5 141.1 %copy-start = (bf16[512,2048]{1,0:T(8,128)(2,1)S(1)}, bf16[512,2048]{1,0:T(8,128)(2,1)}, u32[]{:S(2)}) copy-start(bf16[512,2048]{1,0:T(8,128)(2,1)} %param.34) | copy-start | bytes 6291460
  6.5 3.9 %copy-start.17 = (f32[8]{0:T(128)S(1)}, f32[8]{0:T(128)}, u32[]{:S(2)}) copy-start(f32[8]{0:T(128)} %param.26) | copy-start | bytes 100
  6.5 35.2 %copy-start.11 = (f32[768,2]{0,1:T(2,128)S(1)}, f32[768,2]{0,1:T(2,128)}, u32[]{:S(2)}) copy-start(f32[768,2]{0,1:T(2,128)} %param.27) | copy-start | bytes 18436
  6.5 35.2 %all-gather.6.cloned.1.call-start = ((), (), s32[]{:S(2)}) async-start(), calls=%async_computation.1 | async-start | bytes 3932160 | tf_op jit(solution)/shard_map/all_gather | solution.py:85
  10.4 120.2 %all-gather.8.cloned.1.call-start = ((), (), s32[]{:S(2)}) async-start(), calls=%async_computation.3 | async-start | bytes 2359296 | tf_op jit(solution)/shard_map/all_gather | solution.py:25
  45.8 3.2 %copy-start.1 = (bf16[768,2048]{1,0:T(8,128)(2,1)S(1)}, bf16[768,2048]{1,0:T(8,128)(2,1)}, u32[]{:S(2)}) copy-start(bf16[768,2048]{1,0:T(8,128)(2,1)} %all-gather.6.cloned.1.call-done) | copy-start | bytes 9437188
  45.8 3.5 %copy-start.13 = (bf16[2048,512]{1,0:T(8,128)(2,1)S(1)}, bf16[2048,512]{1,0:T(8,128)(2,1)}, u32[]{:S(2)}) copy-start(bf16[2048,512]{1,0:T(8,128)(2,1)} %param.23) | copy-start | bytes 6291460
  49.3 1.9 copy-start.6
  51.2 1.1 copy-start.7
  51.2 3.1 %copy-start.18 = (u32[32]{0:T(128)S(1)}, u32[32]{0:T(128)}, u32[]{:S(2)}) copy-start(u32[32]{0:T(128)} %constant.70) | copy-start | bytes 388
  52.3 0.8 copy-start.5
  54.2 144.0 %reduce-scatter.2.cloned.1.call-start = ((), (), s32[]{:S(2)}) async-start(), calls=%async_computation.2 | async-start | bytes 3932160 | tf_op jit(solution)/shard_map/reduce_scatter | solution.py:188
  98.3 4.7 %copy-start.10 = (bf16[768,256]{0,1:T(8,128)(2,1)}, bf16[768,256]{0,1:T(8,128)(2,1)S(1)}, u32[]{:S(2)}) copy-start(bf16[768,256]{0,1:T(8,128)(2,1)S(1)} %convolution_convert_fusion.5) | copy-start | bytes 1179652
  98.5 4.5 %copy-start.2 = (bf16[768,2048]{1,0:T(8,128)(2,1)S(1)}, bf16[768,2048]{1,0:T(8,128)(2,1)}, u32[]{:S(2)}) copy-start(bf16[768,2048]{1,0:T(8,128)(2,1)} %all-gather.6.cloned.1.call-done) | copy-start | bytes 9437188
  98.5 4.5 %copy-start.14 = (bf16[2048,512]{1,0:T(8,128)(2,1)S(1)}, bf16[2048,512]{1,0:T(8,128)(2,1)}, u32[]{:S(2)}) copy-start(bf16[2048,512]{1,0:T(8,128)(2,1)} %param.29) | copy-start | bytes 6291460
  104.9 4.2 %copy-start.15 = (bf16[2048,512]{1,0:T(8,128)(2,1)S(1)}, bf16[2048,512]{1,0:T(8,128)(2,1)}, u32[]{:S(2)}) copy-start(bf16[2048,512]{1,0:T(8,128)(2,1)} %param.28) | copy-start | bytes 6291460
  105.1 24.1 %collective-permute-start = (bf16[2,512]{1,0:T(2,128)(2,1)S(1)}, bf16[2,512]{1,0:T(2,128)(2,1)S(1)}, u32[]{:S(2)}, u32[]{:S(2)}) collective-permute-start(bf16[2,512]{1,0:T(2,128)(2,1)S(1)} %slice.42), channel_id=1, source_target_pairs={{0,4},{4,8},{8,12},{12,16},{16,20},{20,24},{24,28},{1,5},{5,9},{9,... | collective-permute-start | bytes 6152 | tf_op jit(solution)/shard_map/ppermute | solution.py:20
  130.8 3.4 %copy-start.8 = (bf16[768,512]{0,1:T(8,128)(2,1)S(1)}, bf16[768,512]{0,1:T(8,128)(2,1)}, u32[]{:S(2)}) copy-start(bf16[768,512]{0,1:T(8,128)(2,1)} %copy-done.7) | copy-start | bytes 2359300
  134.2 2.2 %copy-start.12 = (f32[2,128]{1,0:T(2,128)S(1)}, f32[2,128]{1,0:T(2,128)}, u32[]{:S(2)}) copy-start(f32[2,128]{1,0:T(2,128)} %param.33) | copy-start | bytes 3076
  134.2 3.1 %copy-start.16 = (f32[2,128,256]{2,1,0:T(8,128)S(1)}, f32[2,128,256]{2,1,0:T(8,128)}, u32[]{:S(2)}) copy-start(f32[2,128,256]{2,1,0:T(8,128)} %param.32) | copy-start | bytes 786436
  147.7 1.9 copy-start.3
  147.7 2.1 %copy-start.4 = (bf16[512,2048]{1,0:T(8,128)(2,1)S(1)}, bf16[512,2048]{1,0:T(8,128)(2,1)}, u32[]{:S(2)}) copy-start(bf16[512,2048]{1,0:T(8,128)(2,1)} %param.35) | copy-start | bytes 6291460
  147.7 2.2 %copy-start.9 = (bf16[768,512]{1,0:T(8,128)(2,1)S(1)}, bf16[768,512]{1,0:T(8,128)(2,1)}, u32[]{:S(2)}) copy-start(bf16[768,512]{1,0:T(8,128)(2,1)} %convolution_convert_fusion.2) | copy-start | bytes 2359300
Sparse Core Ops, SparseCore 0:
  10.5 31.2 all-gather.5
  54.3 48.8 all-gather.7
  153.8 44.3 reduce-scatter.1
where the time goes:
time: 205 us
  waiting for transfers between devices  75.8 us (37%)
  blocking collectives  60.6 us (30%)
  matrix products  37.1 us (18%)
  between operations  14.1 us (7%)
  other arithmetic  9.26 us (5%)
  starting transfers between devices  4.02 us (2%)
  local copies, waits for them, and re-layouts  3.93 us (2%)
    reduce_scatter x1, waiting for transfers between devices, per_device(): lax.psum_scatter((jnp.dot(heads_out, w_out_memory, preferred_element_type...  44.5 us
    all_gather x2, blocking collectives, entering(): gathered = jax.tree.map(lambda a: lax.all_gather(a, axis), part)  37 us
    all_gather x1, waiting for transfers between devices, per_device(): sub_rows = lax.all_gather(normed, 'tp', axis=0, tiled=True)  31.2 us
    dot_general x8, matrix products, per_device(): jnp.dot(sub_rows, weight, preferred_element_type=jnp.float32)  21.1 us
    unnamed x1, blocking collectives  17.7 us
    psum x1, blocking collectives, per_device(): row_total = lax.psum(local_squares, 'tp')  5.88 us
  transfers between devices with their start and end apart: 4, of which 2 were waited for; matrix products, arithmetic and copies ran while one was open for 8% of the time, Pallas kernels for 0%

commit v1 on v0

v1 whole, which is shorter than its diff:
```python
import jax
import jax.numpy as jnp
from jax import lax
from jax.experimental import pallas as pl
from jax.experimental.pallas import tpu as pltpu
from jax.sharding import PartitionSpec as P


KEY_DIM = 128
VALUE_DIM = 256
TAPS = 3
CORES = 2
LANES = 128
EDGE = 16
EPSILON = 1e-06
VERY_NEGATIVE = -1e30
QUERY_SCALE = KEY_DIM ** (-0.5)
F32 = jnp.float32
BF16 = jnp.bfloat16


def dot(a, b):
    return jnp.dot(a, b, preferred_element_type=F32)


def shape(rows, columns, dtype):
    return jax.ShapeDtypeStruct((rows, columns), dtype)


def run(body, outs, *args, scalars=0, scratch=(), flops=0, limit=16):
    in_specs = [pl.BlockSpec(memory_space=pltpu.SMEM)] * scalars
    in_specs += [pl.BlockSpec(memory_space=pltpu.VMEM)] * (len(args) - scalars)
    args = [
        a if i < scalars else pltpu.with_memory_space_constraint(a, pltpu.VMEM)
        for i, a in enumerate(args)
    ]
    return pl.pallas_call(
        body,
        out_shape=[pltpu.VMEM(o.shape, o.dtype) for o in outs],
        in_specs=in_specs,
        out_specs=[pl.BlockSpec(memory_space=pltpu.VMEM)] * len(outs),
        scratch_shapes=scratch,
        cost_estimate=pl.CostEstimate(flops=flops, bytes_accessed=0, transcendentals=0),
        compiler_params=pltpu.CompilerParams(vmem_limit_bytes=limit << 20),
    )(*args)


def xor(block, axis, distance):
    return lax.ppermute(block, axis, [(i, i ^ distance) for i in range(lax.axis_size(axis))])


def place(tp, piece, rows):
    return pl.ds(pl.multiple_of(jnp.bitwise_xor(tp, piece) * rows, rows), rows)


def normalize(tokens, gain):
    wide = tokens.astype(F32)
    scale = lax.rsqrt(jnp.mean(wide * wide, axis=1, keepdims=True) + EPSILON)
    return (wide * scale * gain).astype(BF16)


def project_kv(blocks, gain, w_key, w_value, w_gates, normed, kv, gates):
    rows = blocks[0].shape[0]
    width = w_key.shape[1]
    for i, block in enumerate(blocks):
        normed[i * rows : (i + 1) * rows] = normalize(block[...], gain[...])
    gates[...] = dot(normed[...], w_gates[...])
    kv[:, :width] = dot(normed[...], w_key[...]).astype(BF16)
    kv[:, width:] = dot(normed[...], w_value[...]).astype(BF16)


def kv_kernel(*refs):
    project_kv(refs[:-7], *refs[-7:])


def pieces3(x):
    high = x.astype(BF16).astype(F32)
    rest = x - high
    middle = rest.astype(BF16).astype(F32)
    return high, middle, rest - middle


def write_payload(payload, memory, small):
    width = memory.shape[0]
    payload[:width] = memory.astype(BF16)
    high, middle, low = pieces3(small)
    extra = jnp.concatenate(
        [
            jnp.concatenate([high, middle], axis=1),
            jnp.concatenate([low, jnp.zeros_like(low)], axis=1),
        ],
        axis=0,
    )
    payload[width:] = extra.astype(BF16)


def read_payload(payload):
    width = payload.shape[0] - 16
    extra = payload[width:].astype(F32)
    small = extra[:8, :LANES] + extra[:8, LANES:] + extra[8:, :LANES]
    return payload[:width].astype(F32), small


def state_kernel(n_blocks, n_a, n_b, *refs):
    tp_ref, refs = refs[0], refs[1:]
    blocks, refs = refs[:n_blocks], refs[n_blocks:]
    gain, w_key, w_value, w_gates, kv_a, kv_b, gates_a, gates_b, extra, bias = refs[:10]
    normed, kv_all, score_log, memory, small, payload = refs[10:16]
    kv_c, gates_c, gates_all = refs[16:]
    project_kv(blocks, gain, w_key, w_value, w_gates, normed, kv_c, gates_c)
    tp = tp_ref[0]
    rows = blocks[0].shape[0]
    sources = [(i, kv_a, gates_a, i) for i in range(n_a)]
    sources += [(CORES * (i + 1), kv_b, gates_b, i) for i in range(n_b)]
    sources += [(CORES * (i + 1) + 1, kv_c, gates_c, i) for i in range(n_blocks)]
    for piece, kv, gates, at in sources:
        kv_all[place(tp, piece, rows)] = kv[at * rows : (at + 1) * rows]
        gates_all[place(tp, piece, rows)] = gates[at * rows : (at + 1) * rows]
    length = kv_all.shape[0]
    width = w_key.shape[1]
    heads = width // KEY_DIM
    forget = gates_all[:, LANES:] + bias[...]
    log_forget = jnp.minimum(forget, 0.0) - jnp.log1p(jnp.exp(-jnp.abs(forget))) + extra[...]
    row = lax.broadcasted_iota(jnp.int32, (length, length), 0)
    column = lax.broadcasted_iota(jnp.int32, (length, length), 1)
    ones = jnp.where(row >= column, 1.0, 0.0).astype(BF16)
    high, middle, low = pieces3(log_forget)
    cumulative = dot(ones, high.astype(BF16)) + (
        dot(ones, middle.astype(BF16)) + dot(ones, low.astype(BF16))
    )
    score = gates_all[:, :LANES] - cumulative
    score_log[...] = score
    decay = cumulative[length - 1 : length]
    weight_log = decay + score
    block_max = jnp.max(weight_log, axis=0, keepdims=True)
    weight = jnp.exp(weight_log - block_max)
    small[...] = jnp.zeros_like(small)
    small[0:1] = decay
    small[1:2] = block_max
    for h in range(heads):
        keys = slice(h * KEY_DIM, (h + 1) * KEY_DIM)
        values = slice(width + h * VALUE_DIM, width + (h + 1) * VALUE_DIM)
        keyed = kv_all[:, keys].astype(F32) * weight[:, h : h + 1]
        small[2 + h : 3 + h] = jnp.sum(keyed, axis=0, keepdims=True)
        memory[keys] = lax.dot_general(
            keyed.astype(BF16),
            kv_all[:, values],
            (((0,), (0,)), ((), ())),
            preferred_element_type=F32,
        )
    write_payload(payload, memory[...], small[...])


def rest_kernel(normed, w_query, w_gate, w_left, w_right, query, gate, product):
    query[...] = dot(normed[...], w_query[...]).astype(BF16)
    gate[...] = dot(normed[...], w_gate[...]).astype(BF16)
    left = dot(normed[...], w_left[...]).astype(BF16).astype(F32)
    right = dot(normed[...], w_right[...]).astype(BF16).astype(F32)
    product[...] = (left * right).astype(BF16)


def conv_kernel(n_a, n_b, n_c, *refs):
    tp_ref, normed_b, normed_c, edge, gain = refs[:5]
    w_query, w_gate, w_left, w_right, taps, query_a, gate_a, product_a = refs[5:13]
    query_all, branch = refs[13:15]
    normed, gate_all, padded = refs[15:]
    tp = tp_ref[0]
    n = n_b + n_c
    rows = normed_b.shape[0] // n_b
    length = query_all.shape[0]
    normed[: n_b * rows] = normed_b[...]
    normed[n_b * rows : n * rows] = normed_c[...]
    normed[n * rows :] = normalize(edge[...], gain[...])
    order = [CORES * (i + 1) for i in range(n_b)] + [CORES * (i + 1) + 1 for i in range(n_c)]
    query = dot(normed[: n * rows], w_query[...]).astype(BF16)
    gate = dot(normed[: n * rows], w_gate[...])
    left = dot(normed[...], w_left[...]).astype(BF16).astype(F32)
    right = dot(normed[...], w_right[...]).astype(BF16).astype(F32)
    product = (left * right).astype(BF16).astype(F32)
    padded[:EDGE] = product[n * rows :]
    for at, piece in enumerate(order):
        here = slice(at * rows, (at + 1) * rows)
        query_all[place(tp, piece, rows)] = query[here]
        gate_all[place(tp, piece, rows)] = gate[here].astype(BF16)
        start = pl.multiple_of(jnp.bitwise_xor(tp, piece) * rows + EDGE, EDGE)
        padded[pl.ds(start, rows)] = product[here]
    for piece in range(n_a):
        here = slice(piece * rows, (piece + 1) * rows)
        query_all[place(tp, piece, rows)] = query_a[here]
        gate_all[place(tp, piece, rows)] = gate_a[here]
        start = pl.multiple_of(jnp.bitwise_xor(tp, piece) * rows + EDGE, EDGE)
        padded[pl.ds(start, rows)] = product_a[here].astype(F32)
    first = EDGE - (TAPS - 1)
    filtered = taps[0:1] * padded[first : first + length]
    for tap in range(1, TAPS):
        filtered = filtered + taps[tap : tap + 1] * padded[first + tap : first + tap + length]
    branch[...] = (gate_all[...].astype(F32) * filtered).astype(BF16)


def inner_kernel(query, kv, score_log, from_values, row_log, row_sum):
    length, width = query.shape
    heads = width // KEY_DIM
    score_rows = score_log[...].T
    step = 256
    lane = lax.broadcasted_iota(jnp.int32, (step, LANES), 1)
    for first in range(0, length, step):
        last = first + step
        here = slice(first, last)
        logs = jnp.zeros((step, LANES), F32)
        sums = jnp.zeros((step, LANES), F32)
        row = lax.broadcasted_iota(jnp.int32, (step, last), 0) + first
        column = lax.broadcasted_iota(jnp.int32, (step, last), 1)
        for h in range(heads):
            keys = slice(h * KEY_DIM, (h + 1) * KEY_DIM)
            values = slice(width + h * VALUE_DIM, width + (h + 1) * VALUE_DIM)
            raw = lax.dot_general(
                query[here, keys],
                kv[:last, keys],
                (((1,), (1,)), ((), ())),
                preferred_element_type=F32,
            )
            log = jnp.where(row >= column, score_rows[h : h + 1, :last], VERY_NEGATIVE)
            top = jnp.max(log, axis=1, keepdims=True)
            mixing = raw * QUERY_SCALE * jnp.exp(log - top)
            logs = jnp.where(lane == h, top, logs)
            sums = jnp.where(lane == h, jnp.sum(mixing, axis=1, keepdims=True), sums)
            from_values[here, h * VALUE_DIM : (h + 1) * VALUE_DIM] = dot(
                mixing.astype(BF16), kv[:last, values]
            )
        row_log[here] = logs
        row_sum[here] = sums


def scales(early, late):
    top = jnp.maximum(early[1:2] + late[0:1], late[1:2])
    return top, jnp.exp(early[1:2] + late[0:1] - top), jnp.exp(late[1:2] - top)


def join(early_memory, early, late_memory, late, memory, small):
    top, scale_early, scale_late = scales(early, late)
    small[0:1] = early[0:1] + late[0:1]
    small[1:2] = top
    for h in range(memory.shape[0] // KEY_DIM):
        keys = slice(h * KEY_DIM, (h + 1) * KEY_DIM)
        a, b = scale_early[:, h : h + 1], scale_late[:, h : h + 1]
        memory[keys] = a * early_memory[keys] + b * late_memory[keys]
        small[2 + h : 3 + h] = a * early[2 + h : 3 + h] + b * late[2 + h : 3 + h]


def empty(small):
    row = lax.broadcasted_iota(jnp.int32, small.shape, 0)
    return jnp.where(row == 1, VERY_NEGATIVE, 0.0)


def join_kernel(distance, has_prior, *refs):
    sp_ref, total_memory, total_small, received = refs[:4]
    refs = refs[4:]
    if has_prior:
        prior_memory, prior_small = refs[:2]
        refs = refs[2:]
    new_memory, new_small, next_memory, next_small, payload = refs
    late = jnp.bitwise_and(sp_ref[0], distance) != 0
    their_memory, their_small = read_payload(received)

    new_small[...] = jnp.zeros_like(new_small)
    next_small[...] = jnp.zeros_like(next_small)

    @pl.when(late)
    def _():
        join(their_memory, their_small, total_memory, total_small, new_memory, new_small)
        if has_prior:
            join(their_memory, their_small, prior_memory, prior_small, next_memory, next_small)
        else:
            next_memory[...] = their_memory
            next_small[...] = their_small

    @pl.when(jnp.logical_not(late))
    def _():
        join(total_memory, total_small, their_memory, their_small, new_memory, new_small)
        if has_prior:
            next_memory[...] = prior_memory[...]
            next_small[...] = prior_small[...]
        else:
            next_memory[...] = jnp.zeros_like(next_memory)
            next_small[...] = empty(next_small)

    write_payload(payload, new_memory[...], new_small[...])


def memory_kernel(distance, *refs):
    sp_ref, prior_memory, prior_small, received, first_memory, first_norm = refs[:6]
    query, from_values, row_log, row_sum, out, squares = refs[6:12]
    enter_memory, enter_small = refs[12:]
    heads = prior_memory.shape[0] // KEY_DIM
    late = jnp.bitwise_and(sp_ref[0], distance) != 0
    enter_small[...] = jnp.zeros_like(enter_small)

    @pl.when(late)
    def _():
        their_memory, their_small = read_payload(received)
        join(their_memory, their_small, prior_memory, prior_small, enter_memory, enter_small)

    @pl.when(jnp.logical_not(late))
    def _():
        enter_memory[...] = prior_memory[...]
        enter_small[...] = prior_small[...]

    decay, top = enter_small[0:1], enter_small[1:2]
    enter_max = jnp.maximum(top, decay)
    from_prior = jnp.exp(top - enter_max)
    from_first = jnp.exp(decay - enter_max)
    length = query.shape[0]
    total = jnp.zeros((length, 1), F32)
    for h in range(heads):
        keys = slice(h * KEY_DIM, (h + 1) * KEY_DIM)
        values = slice(h * VALUE_DIM, (h + 1) * VALUE_DIM)
        a, b = from_prior[:, h : h + 1], from_first[:, h : h + 1]
        carry_memory = a * enter_memory[keys] + b * first_memory[keys]
        carry_norm = a * enter_small[2 + h : 3 + h] + b * first_norm[h : h + 1]
        high = carry_memory.astype(BF16)
        low = (carry_memory - high.astype(F32)).astype(BF16)
        rows = query[:, keys]
        by_norm = jnp.sum(rows.astype(F32) * carry_norm, axis=1, keepdims=True)
        inner_log = row_log[:, h : h + 1]
        carry_max = enter_max[:, h : h + 1]
        row_max = jnp.maximum(inner_log, carry_max)
        inner = jnp.exp(inner_log - row_max)
        outer = jnp.exp(carry_max - row_max) * QUERY_SCALE
        below = inner * row_sum[:, h : h + 1] + outer * by_norm
        over = 1.0 / jnp.maximum(jnp.abs(below), 1.0)
        by_memory = dot(rows, high) + dot(rows, low)
        result = (inner * over) * from_values[:, values] + (outer * over) * by_memory
        total = total + jnp.sum(result * result, axis=1, keepdims=True)
        out[:, values] = result.astype(BF16)
    squares[...] = jnp.broadcast_to(total, (length, LANES)).T[:8]


def out_kernel(pieces, all_values, *refs):
    tp_ref, memory_out, branch, squares, w_memory, w_conv, keep, send, scale = refs
    tp = tp_ref[0]
    rows = keep.shape[0] * CORES // len(pieces)
    length, width = memory_out.shape[0], keep.shape[1]
    total = jnp.broadcast_to(squares[0:1], (LANES, length)).T
    scale[...] = lax.rsqrt(total / all_values + EPSILON)
    step = 512
    for i, piece in enumerate(pieces):
        here = place(tp, piece, rows)
        to = send if piece % CORES else keep
        at = slice((i // CORES) * rows, (i // CORES + 1) * rows)
        heads = memory_out[here]
        conv = branch[here]
        by = scale[here, 0:1]
        for first in range(0, width, step):
            columns = slice(first, first + step)
            part = by * dot(heads, w_memory[:, columns]) + dot(conv, w_conv[:, columns])
            to[at, columns] = part.astype(BF16)


def per_device(
    tokens,
    in_gain,
    w_query,
    w_key,
    w_value,
    w_input_gate,
    w_forget_gate,
    forget_bias,
    forget_extra,
    w_conv_gate,
    w_conv_left,
    w_conv_right,
    conv_taps,
    first_memory,
    first_norm,
    w_out_memory,
    w_out_conv,
):
    n_tp, n_sp = lax.axis_size("tp"), lax.axis_size("sp")
    n_y = n_tp // CORES
    rows, depth = tokens.shape
    length = rows * n_tp
    width = w_query.shape[1]
    value_width = w_value.shape[1]
    heads = width // KEY_DIM
    channels = w_conv_gate.shape[1]
    tp, sp = lax.axis_index("tp"), lax.axis_index("sp")
    tp_at, sp_at = tp.reshape(1), sp.reshape(1)

    direct = [xor(tokens, "tp", CORES * i) for i in range(1, n_y)]
    partner = xor(tokens, "tp", 1)
    passed = [xor(block, "tp", 1) for block in direct]

    last = n_tp - 1
    edge = lax.ppermute(
        tokens[rows - EDGE :],
        ("sp", "tp"),
        [(s * n_tp + last, (s + 1) * n_tp + last) for s in range(n_sp - 1)],
    )
    edge = edge + lax.ppermute(edge, "tp", [(last, last - 1)])
    ends = [last, last - 1]
    edge_far = [lax.ppermute(edge, "tp", [(a, a - CORES * i) for a in ends]) for i in range(1, n_y)]
    for block in edge_far:
        edge = edge + block

    head_first = tp * heads
    gate_columns = [
        lax.dynamic_slice_in_dim(w, head_first, heads, 1) for w in (w_input_gate, w_forget_gate)
    ]
    pad = ((0, 0), (0, LANES - heads))
    w_gates = jnp.concatenate([jnp.pad(w, pad) for w in gate_columns], axis=1)
    bias = jnp.pad(lax.dynamic_slice_in_dim(forget_bias, head_first, heads, 0)[None], pad)
    extra = jnp.pad(forget_extra, pad)
    gain = in_gain[None]
    taps = lax.dynamic_slice_in_dim(conv_taps, tp * channels, channels, 1)

    def kv_of(blocks):
        n = len(blocks) * rows
        return run(
            kv_kernel,
            [shape(n, depth, BF16), shape(n, width + value_width, BF16), shape(n, 2 * LANES, F32)],
            *blocks,
            gain,
            w_key,
            w_value,
            w_gates,
            flops=2 * n * depth * (width + value_width),
        )

    normed_a, kv_a, gates_a = kv_of([tokens, partner])
    n_a = CORES * rows
    query_a, gate_a, product_a = run(
        rest_kernel,
        [shape(n_a, width, BF16), shape(n_a, channels, BF16), shape(n_a, channels, BF16)],
        normed_a,
        w_query,
        w_conv_gate,
        w_conv_left,
        w_conv_right,
        flops=2 * n_a * depth * (width + 3 * channels),
    )
    normed_b, kv_b, gates_b = kv_of(direct)
    n_c = len(passed) * rows
    normed_c, kv_all, score_log, memory, small, payload = run(
        lambda *refs: state_kernel(len(passed), CORES, len(direct), *refs),
        [
            shape(n_c, depth, BF16),
            shape(length, width + value_width, BF16),
            shape(length, LANES, F32),
            shape(width, VALUE_DIM, F32),
            shape(8, LANES, F32),
            shape(width + 16, VALUE_DIM, BF16),
        ],
        tp_at,
        *passed,
        gain,
        w_key,
        w_value,
        w_gates,
        kv_a,
        kv_b,
        gates_a,
        gates_b,
        extra,
        bias,
        scalars=1,
        scratch=[
            pltpu.VMEM((n_c, width + value_width), BF16),
            pltpu.VMEM((n_c, 2 * LANES), F32),
            pltpu.VMEM((length, 2 * LANES), F32),
        ],
        flops=2 * n_c * depth * (width + value_width),
    )
    n_bc = len(direct + passed) * rows
    query_all, branch = run(
        lambda *refs: conv_kernel(CORES, len(direct), len(passed), *refs),
        [shape(length, width, BF16), shape(length, channels, BF16)],
        tp_at,
        normed_b,
        normed_c,
        edge,
        gain,
        w_query,
        w_conv_gate,
        w_conv_left,
        w_conv_right,
        taps,
        query_a,
        gate_a,
        product_a,
        scalars=1,
        scratch=[
            pltpu.VMEM((n_bc + EDGE, depth), BF16),
            pltpu.VMEM((length, channels), BF16),
            pltpu.VMEM((length + EDGE, channels), F32),
        ],
        flops=2 * n_bc * depth * (width + 3 * channels),
    )
    from_values, row_log, row_sum = run(
        inner_kernel,
        [shape(length, value_width, F32), shape(length, LANES, F32), shape(length, LANES, F32)],
        query_all,
        kv_all,
        score_log,
        flops=2 * heads * length * length * (KEY_DIM + VALUE_DIM),
    )

    prior = ()
    distance = 1
    while distance < n_sp // 2:
        received = xor(payload, "sp", distance)
        memory, small, next_memory, next_small, payload = run(
            lambda *refs, d=distance, p=len(prior) > 0: join_kernel(d, p, *refs),
            [shape(width, VALUE_DIM, F32), shape(8, LANES, F32)] * 2
            + [shape(width + 16, VALUE_DIM, BF16)],
            sp_at,
            memory,
            small,
            received,
            *prior,
            scalars=1,
            flops=8 * width * VALUE_DIM,
        )
        prior = (next_memory, next_small)
        distance *= 2
    received = xor(payload, "sp", distance)
    memory_out, squares = run(
        lambda *refs: memory_kernel(distance, *refs),
        [shape(length, value_width, BF16), shape(8, length, F32)],
        sp_at,
        *prior,
        received,
        first_memory.reshape(width, VALUE_DIM),
        first_norm,
        query_all,
        from_values,
        row_log,
        row_sum,
        scalars=1,
        scratch=[pltpu.VMEM((width, VALUE_DIM), F32), pltpu.VMEM((8, LANES), F32)],
        flops=4 * length * width * VALUE_DIM,
    )

    squares = squares + xor(squares, "tp", 1)
    far = [xor(squares, "tp", CORES * i) for i in range(1, n_y)]
    for block in far:
        squares = squares + block

    def projected(pieces):
        n = len(pieces) // CORES * rows
        return run(
            lambda *refs: out_kernel(pieces, value_width * n_tp, *refs),
            [shape(n, depth, BF16), shape(n, depth, BF16)],
            tp_at,
            memory_out,
            branch,
            squares,
            w_out_memory,
            w_out_conv,
            scalars=1,
            scratch=[pltpu.VMEM((length, LANES), F32)],
            flops=2 * CORES * n * depth * (value_width + channels),
        )

    keep_far, send_far = projected(list(range(CORES, n_tp)))
    pair_far = (keep_far.astype(F32) + xor(send_far, "tp", 1).astype(F32)).astype(BF16)
    arrived = [xor(pair_far[(i - 1) * rows : i * rows], "tp", CORES * i) for i in range(1, n_y)]
    keep_own, send_own = projected(list(range(CORES)))
    mixed = keep_own.astype(F32) + xor(send_own, "tp", 1).astype(F32)
    for block in arrived:
        mixed = mixed + block.astype(F32)
    return mixed.astype(BF16)


def solution(mesh):
    in_specs = (
        P(("sp", "tp"), None),
        P(),
        P(None, "tp"),
        P(None, "tp"),
        P(None, "tp"),
        P(),
        P(),
        P(),
        P("sp", "tp"),
        P(None, "tp"),
        P(None, "tp"),
        P(None, "tp"),
        P(),
        P("tp", None, None),
        P("tp", None),
        P("tp", None),
        P("tp", None),
    )
    out_specs = P(("sp", "tp"), None)
    return jax.shard_map(
        per_device, mesh=mesh, in_specs=in_specs, out_specs=out_specs, check_vma=False
    )
```

time: 205 us -> 110 us (0.54)
  blocking collectives: 60.6 us -> 0 us
  matrix products: 37.1 us -> 0 us
  waiting for transfers between devices: 75.8 us -> 48.3 us
  Pallas kernels: 0 us -> 26.5 us
  between operations: 14.1 us -> 0.33 us
  local copies, waits for them, and re-layouts: 3.93 us -> 16.5 us
  starting transfers between devices: 4.02 us -> 13.5 us
  other arithmetic: 9.26 us -> 3.88 us
    ppermute x1 -> x14, waiting for transfers between devices: 0.01 us -> 48.3 us  [the longest x11 43.5 us: xor(): lax.ppermute(block, axis, [(i, i ^ distance) for i in range(lax.axis_size...]
    reduce_scatter x1 -> x0, waiting for transfers between devices: 44.5 us -> none  [per_device(): lax.psum_scatter((jnp.dot(heads_out, w_out_memory, preferred_element_type...]
    dot_general x15 -> x0, matrix products: 37.1 us -> none  [the longest x8 21.1 us: per_device(): jnp.dot(sub_rows, weight, preferred_element_type=jnp.float32)]
    all_gather x2 -> x0, blocking collectives: 37 us -> none  [entering(): gathered = jax.tree.map(lambda a: lax.all_gather(a, axis), part)]
    all_gather x2 -> x0, waiting for transfers between devices: 31.2 us -> none  [the longest x1 31.2 us: per_device(): sub_rows = lax.all_gather(normed, 'tp', axis=0, tiled=True)]
    pallas_call x0 -> x11, Pallas kernels: none -> 26.5 us  [run(): pl.pallas_call(body, out_shape=[pltpu.VMEM(o.shape, o.dtype) for o in out...]
    unnamed x1 -> x0, blocking collectives: 17.7 us -> none
    unnamed x43 -> x57, local copies, waits for them, and re-layouts: 2.28 us -> 14.8 us
  transfers between devices with their start and end apart: 4 -> 14, of which waited for: 2 -> 7; matrix products, arithmetic and copies ran while one was open for 8% -> 7% of each run, Pallas kernels for 0% -> 20%
where the time goes in v1:
time: 110 us; the launch traced here: 109 us
  waiting for transfers between devices  48.3 us (44%)
  Pallas kernels  26.5 us (24%)
  local copies, waits for them, and re-layouts  16.5 us (15%)
  starting transfers between devices  13.5 us (12%)
  other arithmetic  3.88 us (4%)
    ppermute x11, waiting for transfers between devices, xor(): lax.ppermute(block, axis, [(i, i ^ distance) for i in range(lax.axis_size...  43.5 us
    pallas_call x11, Pallas kernels, run(): pl.pallas_call(body, out_shape=[pltpu.VMEM(o.shape, o.dtype) for o in out...  26.5 us
    unnamed x57, local copies, waits for them, and re-layouts  14.8 us
    ppermute x11, starting transfers between devices, xor(): lax.ppermute(block, axis, [(i, i ^ distance) for i in range(lax.axis_size...  10.2 us
    ppermute x1, waiting for transfers between devices, per_device(): lax.ppermute(edge, 'tp', [(a, a - CORES * i) for a in ends])  4.83 us
  transfers between devices with their start and end apart: 14, of which 7 were waited for; matrix products, arithmetic and copies ran while one was open for 7% of the time, Pallas kernels for 20%

profile of v1, /device:TPU:0, one launch (start us, length us, event | category | flops | bytes accessed | tf_op | source)
XLA Modules:
  0.0 109.0 jit_solution(1814075862900422683)
XLA Ops:
  0.0 3.0 %collective-permute-start = (bf16[192,2048]{1,0:T(8,128)(2,1)}, bf16[192,2048]{1,0:T(8,128)(2,1)}, u32[]{:S(2)}, u32[]{:S(2)}) collective-permute-start(bf16[192,2048]{1,0:T(8,128)(2,1)} %refs_0_.1), channel_id=1, source_target_pairs={{0,2},{1,3},{2,0},{3,1},{4,6},{5,7},{6,4},{7,5},{8,10},{9,11},{10,... | collective-permute-start | bytes 2359304 | tf_op jit(solution)/shard_map/ppermute | solution.py:49
  3.0 17.9 %collective-permute-done.refs_0_ = bf16[192,2048]{1,0:T(8,128)(2,1)} collective-permute-done((bf16[192,2048]{1,0:T(8,128)(2,1)}, bf16[192,2048]{1,0:T(8,128)(2,1)}, u32[]{:S(2)}, u32[]{:S(2)}) %collective-permute-start) | collective-permute-done | bytes 786464 | tf_op jit(solution)/shard_map/ppermute | solution.py:49
  24.3 1.1 copy.22
  25.3 1.6 %copy.20 = f32[768,2]{1,0:T(8,128)} copy(f32[768,2]{0,1:T(2,128)} %param.25) | data formatting | bytes 12288 | tf_op args[8]
  26.9 1.4 %fusion.2.refs_5_.refs_4_ = bf16[2048,256]{1,0:T(8,128)(2,1)S(1)} fusion(bf16[2048,2]{1,0:T(8,128)(2,1)} %copy.22, bf16[2048,2]{1,0:T(8,128)(2,1)} %copy.21), kind=kLoop, calls=%fused_computation.6 | loop fusion | flops 4194304 | bytes 1064960 | tf_op jit(solution)/shard_map/concatenate | solution.py:410
  28.5 1.3 %collective-permute-start.7 = (bf16[16,2048]{1,0:T(8,128)(2,1)S(1)}, bf16[16,2048]{1,0:T(8,128)(2,1)}, u32[]{:S(2)}, u32[]{:S(2)}) collective-permute-start(bf16[16,2048]{1,0:T(8,128)(2,1)S(1)} %collective-permute-done.6), channel_id=1, source_target_pairs={{3,2},{7,6},{11,10},{15,14},{19,18},{23,22},{27,26},{31,30}} | collective-permute-start | bytes 196616 | tf_op jit(solution)/shard_map/ppermute | solution.py:399
  29.8 2.4 %shard_map.164 = (bf16[192,2048]{1,0:T(8,128)(2,1)S(1)}, bf16[192,768]{1,0:T(8,128)(2,1)S(1)}, f32[192,256]{1,0:T(8,128)S(1)}) custom-call(bf16[192,2048]{1,0:T(8,128)(2,1)} %collective-permute-done.refs_0_, f32[1,2048]{1,0:T(1,128)S(1)} %bitcast.7, bf16[2048,256]{1,0:T(8,128)(2,1)S(1)} %copy-done.2, bf16[2048,512]{1,0:T(8,128)(2,1)S(1)} %copy-done.1, ...), custom_call_target="tpu_custom_call" | custom-call | flops 603979776 | tf_op jit(solution)/shard_map/pallas_call | solution.py:37
  33.2 3.3 %shard_map.163 = (bf16[384,2048]{1,0:T(8,128)(2,1)S(1)}, bf16[384,768]{1,0:T(8,128)(2,1)S(1)}, f32[384,256]{1,0:T(8,128)S(1)}) custom-call(bf16[192,2048]{1,0:T(8,128)(2,1)S(1)} %copy-done.3, bf16[192,2048]{1,0:T(8,128)(2,1)} %collective-permute-done.2.refs_1_, f32[1,2048]{1,0:T(1,128)S(1)} %bitcast.8, bf16[2048,256]{1,0:T(8,128)(2,1)S(1)} %copy-done.2, ...), custom_call_target="tpu_custom_call" | custom-call | flops 1207959552 | tf_op jit(solution)/shard_map/pallas_call | solution.py:37
  36.5 5.4 %shard_map.165 = (bf16[192,2048]{1,0:T(8,128)(2,1)S(1)}, bf16[768,768]{1,0:T(8,128)(2,1)S(1)}, f32[768,128]{1,0:T(8,128)S(1)}, f32[256,256]{1,0:T(8,128)S(1)}, f...) custom-call(s32[1]{0:T(128)} %bitcast.refs_0_, bf16[192,2048]{1,0:T(8,128)(2,1)} %collective-permute-done.1.refs_1_, ...), custom_call_target="tpu_custom_call" | custom-call | flops 603979776 | tf_op jit(solution)/shard_map/pallas_call | solution.py:37
  44.6 1.7 %collective-permute-start.3 = (bf16[272,256]{1,0:T(8,128)(2,1)}, bf16[272,256]{1,0:T(8,128)(2,1)S(1)}, u32[]{:S(2)}, u32[]{:S(2)}) collective-permute-start(bf16[272,256]{1,0:T(8,128)(2,1)} %get-tuple-element.45), channel_id=1, source_target_pairs={{0,4},{4,0},{8,12},{12,8},{16,20},{20,16},{24,28},{28,24},{1,5},{5... | collective-permute-start | bytes 417800 | tf_op jit(solution)/shard_map/ppermute | solution.py:49
  47.2 1.3 %collective-permute-start.8 = (bf16[16,2048]{1,0:T(8,128)(2,1)S(1)}, bf16[16,2048]{1,0:T(8,128)(2,1)S(1)}, u32[]{:S(2)}, u32[]{:S(2)}) collective-permute-start(bf16[16,2048]{1,0:T(8,128)(2,1)S(1)} %add.38), channel_id=1, source_target_pairs={{3,1},{2,0},{7,5},{6,4},{11,9},{10,8},{15,13},{14,12},{19,17},{18,... | collective-permute-start | bytes 196616 | tf_op jit(solution)/shard_map/ppermute | solution.py:401
  48.5 4.8 %collective-permute-done.8 = bf16[16,2048]{1,0:T(8,128)(2,1)S(1)} collective-permute-done((bf16[16,2048]{1,0:T(8,128)(2,1)S(1)}, bf16[16,2048]{1,0:T(8,128)(2,1)S(1)}, u32[]{:S(2)}, u32[]{:S(2)}) %collective-permute-start.8) | collective-permute-done | bytes 65568 | tf_op jit(solution)/shard_map/ppermute | solution.py:401
  53.6 1.6 %collective-permute-start.4 = (bf16[272,256]{1,0:T(8,128)(2,1)S(1)}, bf16[272,256]{1,0:T(8,128)(2,1)S(1)}, u32[]{:S(2)}, u32[]{:S(2)}) collective-permute-start(bf16[272,256]{1,0:T(8,128)(2,1)S(1)} %get-tuple-element.48), channel_id=1, source_target_pairs={{0,8},{4,12},{8,0},{12,4},{16,24},{20,28},{24,16},{28,20},{1,9},{5... | collective-permute-start | bytes 417800 | tf_op jit(solution)/shard_map/ppermute | solution.py:49
  55.2 1.6 %copy-done.7 = bf16[2048,512]{1,0:T(8,128)(2,1)S(1)} copy-done((bf16[2048,512]{1,0:T(8,128)(2,1)S(1)}, bf16[2048,512]{1,0:T(8,128)(2,1)}, u32[]{:S(2)}) %copy-start.7) | copy-done | bytes 2097176
  56.8 1.6 %copy-done.9 = bf16[2048,512]{1,0:T(8,128)(2,1)S(1)} copy-done((bf16[2048,512]{1,0:T(8,128)(2,1)S(1)}, bf16[2048,512]{1,0:T(8,128)(2,1)}, u32[]{:S(2)}) %copy-start.9) | copy-done | bytes 2097176
  58.4 1.6 %copy-done.10 = bf16[2048,512]{1,0:T(8,128)(2,1)S(1)} copy-done((bf16[2048,512]{1,0:T(8,128)(2,1)S(1)}, bf16[2048,512]{1,0:T(8,128)(2,1)}, u32[]{:S(2)}) %copy-start.10) | copy-done | bytes 2097176
  60.0 1.4 %copy-done.14 = bf16[384,2048]{1,0:T(8,128)(2,1)S(1)} copy-done((bf16[384,2048]{1,0:T(8,128)(2,1)S(1)}, bf16[384,2048]{1,0:T(8,128)(2,1)}, u32[]{:S(2)}) %copy-start.14) | copy-done | bytes 1572888
  61.4 1.2 %copy-done.17 = bf16[2048,256]{1,0:T(8,128)(2,1)S(1)} copy-done((bf16[2048,256]{1,0:T(8,128)(2,1)S(1)}, bf16[2048,256]{1,0:T(8,128)(2,1)}, u32[]{:S(2)}) %copy-start.17) | copy-done | bytes 1048600
  62.7 3.0 %shard_map.168 = (bf16[384,256]{1,0:T(8,128)(2,1)S(1)}, bf16[384,512]{1,0:T(8,128)(2,1)S(1)}, bf16[384,512]{1,0:T(8,128)(2,1)S(1)}) custom-call(bf16[384,2048]{1,0:T(8,128)(2,1)S(1)} %copy-done.14, bf16[2048,256]{1,0:T(8,128)(2,1)S(1)} %copy-done.17, bf16[2048,512]{1,0:T(8,128)(2,1)S(1)} %copy-done.7, bf16[2048,512]{1,0:T(8,128)(2,1)S(1)} %copy-done.9, ...), custom_call_target="tpu_custom_call" | custom-call | flops 2818572288 | tf_op jit(solution)/shard_map/pallas_call | solution.py:37
  65.7 1.1 shard_map.167
  66.8 3.0 %collective-permute-start.5 = (bf16[272,256]{1,0:T(8,128)(2,1)S(1)}, bf16[272,256]{1,0:T(8,128)(2,1)S(1)}, u32[]{:S(2)}, u32[]{:S(2)}) collective-permute-start(bf16[272,256]{1,0:T(8,128)(2,1)S(1)} %get-tuple-element.53), channel_id=1, source_target_pairs={{0,16},{4,20},{8,24},{12,28},{16,0},{20,4},{24,8},{28,12},{1,17},{... | collective-permute-start | bytes 417800 | tf_op jit(solution)/shard_map/ppermute | solution.py:49
  69.8 4.5 %shard_map.169 = (bf16[768,256]{1,0:T(8,128)(2,1)S(1)}, bf16[768,512]{1,0:T(8,128)(2,1)S(1)}) custom-call(s32[1]{0:T(128)} %bitcast.refs_0_, bf16[192,2048]{1,0:T(8,128)(2,1)S(1)} %copy-done.20, bf16[192,2048]{1,0:T(8,128)(2,1)S(1)} %copy-done.22, bf16[16,2048]{1,0:T(8,128)(2,1)S(1)} %add.39.refs_3_, f32[1,2048]{1,0:T(1,128)S(1)} %bitcast.10, ...), custom_call_target="tpu_custom_call" | custom-call | flops 2818572288 | tf_op jit(solution)/shard_map/pallas_call | solution.py:37
  74.4 1.5 %shard_map.170 = (f32[768,512]{1,0:T(8,128)S(1)}, f32[768,128]{1,0:T(8,128)S(1)}, f32[768,128]{1,0:T(8,128)S(1)}) custom-call(bf16[768,256]{1,0:T(8,128)(2,1)S(1)} %get-tuple-element.60.query.refs_6_, bf16[768,768]{1,0:T(8,128)(2,1)S(1)} %copy-done.16, f32[768,128]{1,0:T(8,128)S(1)} %copy-done.24), custom_call_target="tpu_custom_call" | custom-call | flops 905969664 | tf_op jit(solution)/shard_map/pallas_call | solution.py:37
  75.9 1.2 %collective-permute-done.5.refs_3_ = bf16[272,256]{1,0:T(8,128)(2,1)S(1)} collective-permute-done((bf16[272,256]{1,0:T(8,128)(2,1)S(1)}, bf16[272,256]{1,0:T(8,128)(2,1)S(1)}, u32[]{:S(2)}, u32[]{:S(2)}) %collective-permute-start.5) | collective-permute-done | bytes 139296 | tf_op jit(solution)/shard_map/ppermute | solution.py:49
  77.1 1.3 %shard_map.171 = (bf16[768,512]{1,0:T(8,128)(2,1)S(1)}, f32[8,768]{1,0:T(8,128)S(1)}) custom-call(s32[1]{0:T(128)} %bitcast.1.refs_0_, f32[256,256]{1,0:T(8,128)S(1)} %get-tuple-element.51.refs_1_, f32[8,128]{1,0:T(8,128)S(1)} %get-tuple-element.52.refs_2_, bf16[272,256]{1,0:T(8,128)(2,1)S(1)} %collective-permute-done.5.refs_3_, f32[256,256]{1,0:T(8,128)S(1)} %bitcast.6, ...), custom_call_target="tpu_custom_call" | custom-call | flops 201326592 | tf_op jit(solution)/shard_map/pallas_call | solution.py:37
  78.6 1.1 collective-permute-done.9
  79.7 3.8 %collective-permute-done.10 = f32[8,768]{1,0:T(8,128)S(1)} collective-permute-done((f32[8,768]{1,0:T(8,128)S(1)}, f32[8,768]{1,0:T(8,128)S(1)}, u32[]{:S(2)}, u32[]{:S(2)}) %collective-permute-start.10) | collective-permute-done | bytes 24608 | tf_op jit(solution)/shard_map/ppermute | solution.py:49
  83.6 1.9 %shard_map.173 = (bf16[192,2048]{1,0:T(8,128)(2,1)S(1)}, bf16[192,2048]{1,0:T(8,128)(2,1)S(1)}) custom-call(s32[1]{0:T(128)} %bitcast.refs_0_, bf16[768,512]{1,0:T(8,128)(2,1)S(1)} %get-tuple-element.66.refs_1_, bf16[768,512]{1,0:T(8,128)(2,1)S(1)} %get-tuple-element.67.refs_2_, f32[8,768]{1,0:T(8,128)S(1)} %add.42.refs_3_, ...), custom_call_target="tpu_custom_call" | custom-call | flops 1610612736 | tf_op jit(solution)/shard_map/pallas_call | solution.py:37
  85.5 1.9 %shard_map.172 = (bf16[192,2048]{1,0:T(8,128)(2,1)S(1)}, bf16[192,2048]{1,0:T(8,128)(2,1)S(1)}) custom-call(s32[1]{0:T(128)} %bitcast.refs_0_, bf16[768,512]{1,0:T(8,128)(2,1)S(1)} %get-tuple-element.66.refs_1_, bf16[768,512]{1,0:T(8,128)(2,1)S(1)} %get-tuple-element.67.refs_2_, f32[8,768]{1,0:T(8,128)S(1)} %add.42.refs_3_, ...), custom_call_target="tpu_custom_call" | custom-call | flops 1610612736 | tf_op jit(solution)/shard_map/pallas_call | solution.py:37
  88.3 1.6 %collective-permute-done.11 = bf16[192,2048]{1,0:T(8,128)(2,1)S(1)} collective-permute-done((bf16[192,2048]{1,0:T(8,128)(2,1)S(1)}, bf16[192,2048]{1,0:T(8,128)(2,1)S(1)}, u32[]{:S(2)}, u32[]{:S(2)}) %collective-permute-start.11) | collective-permute-done | bytes 786464 | tf_op jit(solution)/shard_map/ppermute | solution.py:49
  89.8 17.9 %collective-permute-done.13 = bf16[192,2048]{1,0:T(8,128)(2,1)S(1)} collective-permute-done((bf16[192,2048]{1,0:T(8,128)(2,1)S(1)}, bf16[192,2048]{1,0:T(8,128)(2,1)S(1)}, u32[]{:S(2)}, u32[]{:S(2)}) %collective-permute-start.13) | collective-permute-done | bytes 786464 | tf_op jit(solution)/shard_map/ppermute | solution.py:49
  107.7 1.3 %add_convert_fusion = bf16[192,2048]{1,0:T(8,128)(2,1)} fusion(bf16[192,2048]{1,0:T(8,128)(2,1)S(1)} %collective-permute-done.13, bf16[192,2048]{1,0:T(8,128)(2,1)S(1)} %collective-permute-done.11, bf16[192,2048]{1,0:T(8,128)(2,1)S(1)} %get-tuple-element.69), kind=kLoop, calls=%fused_computation.4 | loop fusion | flops 2359296 | bytes 3145728 | tf_op jit(solution)/shard_map/convert_element_type | solution.py:571
  (77 shorter events, 9.4 us)
Async XLA Ops:
  0.0 48.5 %copy-start = (f32[3,2048]{1,0:T(4,128)S(1)}, f32[3,2048]{1,0:T(4,128)}, u32[]{:S(2)}) copy-start(f32[3,2048]{1,0:T(4,128)} %param.29) | copy-start | bytes 73732
  0.0 28.4 %copy-start.26 = (f32[8]{0:T(128)S(1)}, f32[8]{0:T(128)}, u32[]{:S(2)}) copy-start(f32[8]{0:T(128)} %param.24) | copy-start | bytes 100
  0.0 20.9 %collective-permute-start = (bf16[192,2048]{1,0:T(8,128)(2,1)}, bf16[192,2048]{1,0:T(8,128)(2,1)}, u32[]{:S(2)}, u32[]{:S(2)}) collective-permute-start(bf16[192,2048]{1,0:T(8,128)(2,1)} %refs_0_.1), channel_id=1, source_target_pairs={{0,2},{1,3},{2,0},{3,1},{4,6},{5,7},{6,4},{7,5},{8,10},{9,11},{10,... | collective-permute-start | bytes 2359304 | tf_op jit(solution)/shard_map/ppermute | solution.py:49
  3.0 30.2 %collective-permute-start.2 = (bf16[192,2048]{1,0:T(8,128)(2,1)}, bf16[192,2048]{1,0:T(8,128)(2,1)}, u32[]{:S(2)}, u32[]{:S(2)}) collective-permute-start(bf16[192,2048]{1,0:T(8,128)(2,1)} %refs_0_.1), channel_id=1, source_target_pairs={{0,1},{1,0},{2,3},{3,2},{4,5},{5,4},{6,7},{7,6},{8,9},{9,8},{10,11... | collective-permute-start | bytes 2359304 | tf_op jit(solution)/shard_map/ppermute | solution.py:49
  20.9 15.7 %collective-permute-start.1 = (bf16[192,2048]{1,0:T(8,128)(2,1)}, bf16[192,2048]{1,0:T(8,128)(2,1)}, u32[]{:S(2)}, u32[]{:S(2)}) collective-permute-start(bf16[192,2048]{1,0:T(8,128)(2,1)} %collective-permute-done.refs_0_), channel_id=1, source_target_pairs={{0,1},{1,0},{2,3},{3,2},{4,5},{5,4},{6,7},{7,6},{8,9},{9,8},{10,11... | collective-permute-start | bytes 2359304 | tf_op jit(solution)/shard_map/ppermute | solution.py:49
  21.7 6.8 %collective-permute-start.6 = (bf16[16,2048]{1,0:T(8,128)(2,1)S(1)}, bf16[16,2048]{1,0:T(8,128)(2,1)S(1)}, u32[]{:S(2)}, u32[]{:S(2)}) collective-permute-start(bf16[16,2048]{1,0:T(8,128)(2,1)S(1)} %slice.3), channel_id=1, source_target_pairs={{3,7},{7,11},{11,15},{15,19},{19,23},{23,27},{27,31}} | collective-permute-start | bytes 196616 | tf_op jit(solution)/shard_map/ppermute | solution.py:394
  23.2 6.6 %copy-start.1 = (bf16[2048,512]{1,0:T(8,128)(2,1)S(1)}, bf16[2048,512]{1,0:T(8,128)(2,1)}, u32[]{:S(2)}) copy-start(bf16[2048,512]{1,0:T(8,128)(2,1)} %refs_4_.5) | copy-start | bytes 6291460
  23.2 6.6 %copy-start.2 = (bf16[2048,256]{1,0:T(8,128)(2,1)S(1)}, bf16[2048,256]{1,0:T(8,128)(2,1)}, u32[]{:S(2)}) copy-start(bf16[2048,256]{1,0:T(8,128)(2,1)} %refs_3_.5) | copy-start | bytes 3145732
  23.2 6.6 %copy-start.5 = (f32[2048]{0:T(1024)S(1)}, f32[2048]{0:T(1024)}, u32[]{:S(2)}) copy-start(f32[2048]{0:T(1024)} %param.18) | copy-start | bytes 24580
  28.5 17.8 %collective-permute-start.7 = (bf16[16,2048]{1,0:T(8,128)(2,1)S(1)}, bf16[16,2048]{1,0:T(8,128)(2,1)}, u32[]{:S(2)}, u32[]{:S(2)}) collective-permute-start(bf16[16,2048]{1,0:T(8,128)(2,1)S(1)} %collective-permute-done.6), channel_id=1, source_target_pairs={{3,2},{7,6},{11,10},{15,14},{19,18},{23,22},{27,26},{31,30}} | collective-permute-start | bytes 196616 | tf_op jit(solution)/shard_map/ppermute | solution.py:399
  29.8 3.3 %copy-start.3 = (bf16[192,2048]{1,0:T(8,128)(2,1)S(1)}, bf16[192,2048]{1,0:T(8,128)(2,1)}, u32[]{:S(2)}) copy-start(bf16[192,2048]{1,0:T(8,128)(2,1)} %refs_0_.1) | copy-start | bytes 2359300
  36.5 5.4 %copy-start.13 = (bf16[384,2048]{1,0:T(8,128)(2,1)}, bf16[384,2048]{1,0:T(8,128)(2,1)S(1)}, u32[]{:S(2)}) copy-start(bf16[384,2048]{1,0:T(8,128)(2,1)S(1)} %get-tuple-element.56.normed) | copy-start | bytes 4718596
  44.6 8.8 %collective-permute-start.3 = (bf16[272,256]{1,0:T(8,128)(2,1)}, bf16[272,256]{1,0:T(8,128)(2,1)S(1)}, u32[]{:S(2)}, u32[]{:S(2)}) collective-permute-start(bf16[272,256]{1,0:T(8,128)(2,1)} %get-tuple-element.45), channel_id=1, source_target_pairs={{0,4},{4,0},{8,12},{12,8},{16,20},{20,16},{24,28},{28,24},{1,5},{5... | collective-permute-start | bytes 417800 | tf_op jit(solution)/shard_map/ppermute | solution.py:49
  47.2 6.2 %collective-permute-start.8 = (bf16[16,2048]{1,0:T(8,128)(2,1)S(1)}, bf16[16,2048]{1,0:T(8,128)(2,1)S(1)}, u32[]{:S(2)}, u32[]{:S(2)}) collective-permute-start(bf16[16,2048]{1,0:T(8,128)(2,1)S(1)} %add.38), channel_id=1, source_target_pairs={{3,1},{2,0},{7,5},{6,4},{11,9},{10,8},{15,13},{14,12},{19,17},{18,... | collective-permute-start | bytes 196616 | tf_op jit(solution)/shard_map/ppermute | solution.py:401
  53.6 12.1 %collective-permute-start.4 = (bf16[272,256]{1,0:T(8,128)(2,1)S(1)}, bf16[272,256]{1,0:T(8,128)(2,1)S(1)}, u32[]{:S(2)}, u32[]{:S(2)}) collective-permute-start(bf16[272,256]{1,0:T(8,128)(2,1)S(1)} %get-tuple-element.48), channel_id=1, source_target_pairs={{0,8},{4,12},{8,0},{12,4},{16,24},{20,28},{24,16},{28,20},{1,9},{5... | collective-permute-start | bytes 417800 | tf_op jit(solution)/shard_map/ppermute | solution.py:49
  56.8 1.6 %copy-start.9 = (bf16[2048,512]{1,0:T(8,128)(2,1)S(1)}, bf16[2048,512]{1,0:T(8,128)(2,1)}, u32[]{:S(2)}) copy-start(bf16[2048,512]{1,0:T(8,128)(2,1)} %refs_7_.1) | copy-start | bytes 6291460
  62.6 7.1 %copy-start.8 = (bf16[2048,512]{1,0:T(8,128)(2,1)S(1)}, bf16[2048,512]{1,0:T(8,128)(2,1)}, u32[]{:S(2)}) copy-start(bf16[2048,512]{1,0:T(8,128)(2,1)} %refs_6_.1) | copy-start | bytes 6291460
  62.6 7.1 %copy-start.18 = (bf16[2048,256]{1,0:T(8,128)(2,1)S(1)}, bf16[2048,256]{1,0:T(8,128)(2,1)}, u32[]{:S(2)}) copy-start(bf16[2048,256]{1,0:T(8,128)(2,1)} %refs_5_.4) | copy-start | bytes 3145732
  62.6 7.1 %copy-start.20 = (bf16[192,2048]{1,0:T(8,128)(2,1)S(1)}, bf16[192,2048]{1,0:T(8,128)(2,1)}, u32[]{:S(2)}) copy-start(bf16[192,2048]{1,0:T(8,128)(2,1)} %copy-done.19) | copy-start | bytes 2359300
  62.7 7.1 %copy-start.22 = (bf16[192,2048]{1,0:T(8,128)(2,1)S(1)}, bf16[192,2048]{1,0:T(8,128)(2,1)}, u32[]{:S(2)}) copy-start(bf16[192,2048]{1,0:T(8,128)(2,1)} %copy-done.21) | copy-start | bytes 2359300
  66.8 10.4 %collective-permute-start.5 = (bf16[272,256]{1,0:T(8,128)(2,1)S(1)}, bf16[272,256]{1,0:T(8,128)(2,1)S(1)}, u32[]{:S(2)}, u32[]{:S(2)}) collective-permute-start(bf16[272,256]{1,0:T(8,128)(2,1)S(1)} %get-tuple-element.53), channel_id=1, source_target_pairs={{0,16},{4,20},{8,24},{12,28},{16,0},{20,4},{24,8},{28,12},{1,17},{... | collective-permute-start | bytes 417800 | tf_op jit(solution)/shard_map/ppermute | solution.py:49
  69.8 4.6 %copy-start.16 = (bf16[768,768]{1,0:T(8,128)(2,1)S(1)}, bf16[768,768]{1,0:T(8,128)(2,1)}, u32[]{:S(2)}) copy-start(bf16[768,768]{1,0:T(8,128)(2,1)} %copy-done.15) | copy-start | bytes 3538948
  69.8 4.6 %copy-start.24 = (f32[768,128]{1,0:T(8,128)S(1)}, f32[768,128]{1,0:T(8,128)}, u32[]{:S(2)}) copy-start(f32[768,128]{1,0:T(8,128)} %copy-done.23) | copy-start | bytes 1179652
  74.3 2.8 %copy-start.4 = (f32[2,128,256]{2,1,0:T(8,128)S(1)}, f32[2,128,256]{2,1,0:T(8,128)}, u32[]{:S(2)}) copy-start(f32[2,128,256]{2,1,0:T(8,128)} %param.30) | copy-start | bytes 786436
  74.3 2.8 %copy-start.6 = (f32[2,128]{1,0:T(2,128)S(1)}, f32[2,128]{1,0:T(2,128)}, u32[]{:S(2)}) copy-start(f32[2,128]{1,0:T(2,128)} %refs_5_.5) | copy-start | bytes 3076
  74.4 9.2 %copy-start.12 = (bf16[512,2048]{1,0:T(8,128)(2,1)S(1)}, bf16[512,2048]{1,0:T(8,128)(2,1)}, u32[]{:S(2)}) copy-start(bf16[512,2048]{1,0:T(8,128)(2,1)} %refs_5_.7) | copy-start | bytes 6291460
  75.8 7.7 %copy-start.11 = (bf16[512,2048]{1,0:T(8,128)(2,1)S(1)}, bf16[512,2048]{1,0:T(8,128)(2,1)}, u32[]{:S(2)}) copy-start(bf16[512,2048]{1,0:T(8,128)(2,1)} %refs_4_.7) | copy-start | bytes 6291460
  78.5 1.2 %collective-permute-start.9 = (f32[8,768]{1,0:T(8,128)S(1)}, f32[8,768]{1,0:T(8,128)S(1)}, u32[]{:S(2)}, u32[]{:S(2)}) collective-permute-start(f32[8,768]{1,0:T(8,128)S(1)} %get-tuple-element.68), channel_id=1, source_target_pairs={{0,1},{1,0},{2,3},{3,2},{4,5},{5,4},{6,7},{7,6},{8,9},{9,8},{10,11... | collective-permute-start | bytes 73736 | tf_op jit(solution)/shard_map/ppermute | solution.py:49
  79.7 3.8 %collective-permute-start.10 = (f32[8,768]{1,0:T(8,128)S(1)}, f32[8,768]{1,0:T(8,128)S(1)}, u32[]{:S(2)}, u32[]{:S(2)}) collective-permute-start(f32[8,768]{1,0:T(8,128)S(1)} %add.41), channel_id=1, source_target_pairs={{0,2},{1,3},{2,0},{3,1},{4,6},{5,7},{6,4},{7,5},{8,10},{9,11},{10,... | collective-permute-start | bytes 73736 | tf_op jit(solution)/shard_map/ppermute | solution.py:49
  85.4 2.5 %collective-permute-start.12 = (bf16[192,2048]{1,0:T(8,128)(2,1)S(1)}, bf16[192,2048]{1,0:T(8,128)(2,1)S(1)}, u32[]{:S(2)}, u32[]{:S(2)}) collective-permute-start(bf16[192,2048]{1,0:T(8,128)(2,1)S(1)} %get-tuple-element.72), channel_id=1, source_target_pairs={{0,1},{1,0},{2,3},{3,2},{4,5},{5,4},{6,7},{7,6},{8,9},{9,8},{10,11... | collective-permute-start | bytes 2359304 | tf_op jit(solution)/shard_map/ppermute | solution.py:49
  87.4 2.5 %collective-permute-start.11 = (bf16[192,2048]{1,0:T(8,128)(2,1)S(1)}, bf16[192,2048]{1,0:T(8,128)(2,1)S(1)}, u32[]{:S(2)}, u32[]{:S(2)}) collective-permute-start(bf16[192,2048]{1,0:T(8,128)(2,1)S(1)} %get-tuple-element.70), channel_id=1, source_target_pairs={{0,1},{1,0},{2,3},{3,2},{4,5},{5,4},{6,7},{7,6},{8,9},{9,8},{10,11... | collective-permute-start | bytes 2359304 | tf_op jit(solution)/shard_map/ppermute | solution.py:49
  88.2 19.5 %collective-permute-start.13 = (bf16[192,2048]{1,0:T(8,128)(2,1)S(1)}, bf16[192,2048]{1,0:T(8,128)(2,1)S(1)}, u32[]{:S(2)}, u32[]{:S(2)}) collective-permute-start(bf16[192,2048]{1,0:T(8,128)(2,1)S(1)} %add_convert_fusion.1), channel_id=1, source_target_pairs={{0,2},{1,3},{2,0},{3,1},{4,6},{5,7},{6,4},{7,5},{8,10},{9,11},{10,... | collective-permute-start | bytes 2359304 | tf_op jit(solution)/shard_map/ppermute | solution.py:49
  (9 other events, 10.9 us)
